TPU v7x, 256 devices: a 4x2x16 block of a 4x16x16 slice. The times are simulated.
256 devices in a mesh: grp: 2 (over y), sp: 32 (over z, core), tp: 4 (over x).
Axes of the slice: x: 4, y: 2, z: 16, core: 2. Of those that a mesh axis runs over, the one named last changes fastest.
The devices are a block of a 4x16x16 slice.
Arguments:
- gate_in: bfloat16 [32768, 1536], P(('grp', 'sp'), 'tp'), parts along dimension 0, may hold values from -6 to 6
- mult_in: bfloat16 [32768, 1536], P(('grp', 'sp'), 'tp'), parts along dimension 0, may hold values from -6 to 6
- value_in: bfloat16 [32768, 1536], P(('grp', 'sp'), 'tp'), parts along dimension 0, may hold values from -6 to 6
- doc_ids: int32 [32768], P(('grp', 'sp')), parts along dimension 0, may hold values from 0 to 15, never falling along the last dimension, each value on 1 to 1536 neighbouring positions
- conv_taps: bfloat16 [3, 1536], P(None, 'tp'), may hold values from -3 to 3
- out_proj: bfloat16 [1536, 2048], P('tp'), may hold values from -0.15625 to 0.15625
- resid: bfloat16 [32768, 2048], P(('grp', 'sp', 'tp')), parts along dimension 0, may hold values from -6 to 6
- norm1_gain: float32 [2048], replicated, may hold values from 0.1 to 1.9
- norm1_bias: float32 [2048], replicated, may hold values from -1.5 to 1.5
- expert_ids: int32 [32768, 2], P(('grp', 'sp', 'tp')), parts along dimension 0, may hold values from 0 to 31, all different within a row; in each aligned block of 128 rows (0 to 127, 128 to 255, ...) at most 10 rows name the same one
- expert_wts: float32 [32768, 2], P(('grp', 'sp', 'tp')), parts along dimension 0, may hold values from 0.1 to 1
- w_gate: bfloat16 [32, 2048, 3072], P('sp', None, 'tp'), may hold values from -0.125 to 0.125
- w_up: bfloat16 [32, 2048, 3072], P('sp', None, 'tp'), may hold values from -0.125 to 0.125
- w_down: bfloat16 [32, 3072, 2048], P('sp', 'tp'), may hold values from -0.21582031 to 0.21582031
- norm2_gain: float32 [2048], replicated, may hold values from 0.1 to 1.9
- norm2_bias: float32 [2048], replicated, may hold values from -1.5 to 1.5
Outputs:
- result: bfloat16 [32768, 2048], P(('grp', 'sp', 'tp')), parts along dimension 0
There are 2 independent parts, one for each index of `grp`. A program takes and returns all parts, laid end to end along the dimension named above; an argument that names none is the same for every part. Nothing has to cross between parts.
Inputs may be any that keep to these rules, and one draw needn't show every extreme that they name: `doc_ids`: never falling along the sequence; each document has 1 to 1536 positions and one has exactly 1536. `expert_ids`: each row names 2 different experts. Among the rows of one device no expert is named more than 10 times, and in some device's rows some expert is named exactly 10 times.
All inputs are finite; a program needn't handle non-finite values.
Results may differ from a plain program's by a relative error of at most 0.0095.
Values may be sent and summed in bfloat16 or wider, within the bound.
No kernel may reach another device: no remote copies, remote signals or barrier semaphores. Data moves between devices by JAX's collectives and lax.ppermute only.
A program may use at most 128 MiB of HBM per device.

v0:
```python
import jax
import jax.numpy as jnp
from jax import lax
from jax.sharding import Mesh
from jax.sharding import PartitionSpec as P

SP = ("sp_0", "sp_1")
GRP_SP = ("grp", "sp_0", "sp_1")
GRP_SP_TP = ("grp", "sp_0", "sp_1", "tp")
SUBLANES = 8
residual_scale = 2.0**0.5
norm_eps = 1e-05


def next_in_sequence(x):
    length = lax.axis_size(SP)
    return lax.ppermute(x, SP, [(i, i + 1) for i in range(length - 1)])


def swapped(x):
    return lax.ppermute(x, "sp_1", [(0, 1), (1, 0)])


def layer_norm(pre, gain, bias):
    center = pre - jnp.mean(pre, axis=-1, keepdims=True)
    spread = jnp.mean(center * center, axis=-1, keepdims=True)
    return center * lax.rsqrt(spread + norm_eps) * gain + bias


def dot(a, b):
    return jnp.dot(a, b, preferred_element_type=jnp.float32)


def chunk_slots(capacity, cores):
    width = SUBLANES // cores
    rest = capacity % width
    sizes = ([rest] if rest else []) + [width] * (capacity // width)
    starts = [sum(sizes[:i]) for i in range(len(sizes))]
    return list(zip(starts, sizes))


def shards(
    gate_in,
    mult_in,
    value_in,
    doc_ids,
    conv_taps,
    out_proj,
    resid,
    norm1_gain,
    norm1_bias,
    expert_ids,
    expert_wts,
    w_gate,
    w_up,
    w_down,
    norm2_gain,
    norm2_bias,
):
    n_tp = lax.axis_size("tp")
    chips = lax.axis_size("sp_0")
    cores = lax.axis_size("sp_1")
    experts = chips * cores
    tok_count, top_count = expert_ids.shape
    width = out_proj.shape[1]
    capacity = 5 * tok_count * top_count // (4 * experts)
    tap_weights = conv_taps.astype(jnp.float32)
    taps = tap_weights.shape[0]
    product = mult_in.astype(jnp.float32) * value_in.astype(jnp.float32)
    docs = doc_ids.astype(jnp.float32)
    row_count, channels = product.shape
    tail_docs = jnp.broadcast_to(docs[row_count - taps + 1 :, None], (taps - 1, channels))
    prev = next_in_sequence(jnp.concatenate([product[row_count - taps + 1 :], tail_docs], axis=0))
    prev_rows, prev_docs = (prev[: taps - 1], prev[taps - 1 :, 0])
    meta = jnp.concatenate([expert_ids.astype(jnp.float32).T, expert_wts.T], axis=0)
    metas = jnp.stack([meta, swapped(meta)])
    ext_rows = jnp.concatenate([prev_rows, product], axis=0)
    ext_docs = jnp.concatenate([prev_docs, docs], axis=0)
    filtered = jnp.zeros_like(product)
    for tap_index in range(taps):
        shifted = ext_rows[tap_index : tap_index + row_count]
        same_doc = (ext_docs[tap_index : tap_index + row_count] == docs)[:, None]
        filtered = filtered + tap_weights[tap_index] * jnp.where(same_doc, shifted, 0.0)
    mixed_heads = (gate_in.astype(jnp.float32) * filtered).astype(jnp.bfloat16)
    partial = dot(mixed_heads, out_proj).astype(jnp.bfloat16)
    partials = lax.all_to_all(
        partial.reshape(n_tp, row_count // n_tp, width), "tp", 0, 0, tiled=True
    )
    mixed = jnp.sum(partials.astype(jnp.float32), axis=0)
    hidden_one = layer_norm(
        residual_scale * resid.astype(jnp.float32) + mixed, norm1_gain, norm1_bias
    ).astype(jnp.bfloat16)
    hidden_both = jnp.concatenate([hidden_one, swapped(hidden_one)], axis=0)
    ids, wts = (metas[:, :top_count], metas[:, top_count:])
    numbers = (jnp.arange(chips) * cores + lax.axis_index("sp_1")).astype(jnp.float32)
    named = ids[:, :, None, :] == numbers[None, None, :, None]
    chosen = jnp.any(named, axis=1)
    weight = jnp.sum(jnp.where(named, wts[:, :, None, :], 0.0), axis=1)
    before = (jnp.arange(tok_count)[:, None] < jnp.arange(tok_count)[None, :]).astype(jnp.bfloat16)
    earlier = dot(chosen.astype(jnp.bfloat16), before)
    slot_of = jnp.where(chosen, earlier, -1.0)

    def selected(start, size, values):
        slots = (start + jnp.arange(size)).astype(jnp.float32)
        hit = slot_of.transpose(1, 0, 2)[:, :, None, None, :] == slots[None, None, :, None, None]
        same = jnp.arange(cores)[:, None] == jnp.arange(cores)[None, :]
        hit = hit & same[None, :, None, :, None]
        picked = jnp.where(hit, values.transpose(1, 0, 2)[:, :, None, None, :], 0.0)
        return picked.reshape(chips * cores * size, cores * tok_count)

    chunks = chunk_slots(capacity, cores)
    ones = jnp.ones_like(weight)
    packed = [
        dot(selected(start, size, ones).astype(jnp.bfloat16), hidden_both)
        .astype(jnp.bfloat16)
        .reshape(chips, cores * size, width)
        for start, size in chunks
    ]
    gathered = []
    for i in range(len(chunks)):
        moved = lax.all_to_all(packed[i], "sp_0", 0, 0, tiled=True)
        rest = tuple(packed[i + 1 :])
        moved, rest = lax.optimization_barrier((moved, rest))
        packed[i + 1 :] = list(rest)
        gathered.append(lax.all_gather(moved.reshape(-1, width), "tp", axis=0, tiled=True))
    scattered = []
    for rows_in in gathered:
        gate_act = dot(rows_in, w_gate[0])
        up_act = dot(rows_in, w_up[0])
        hid = (jax.nn.silu(gate_act) * up_act).astype(jnp.bfloat16)
        piece = dot(hid, w_down[0]).astype(jnp.bfloat16)
        scattered.append(lax.psum_scatter(piece, "tp", scatter_dimension=0, tiled=True))
    total = jnp.zeros((cores * tok_count, width), jnp.float32)
    for i, (start, size) in enumerate(chunks):
        ready = scattered[i].reshape(chips, cores * size, width)
        back = lax.all_to_all(ready, "sp_0", 0, 0, tiled=True).reshape(-1, width)
        factor = selected(start, size, weight)
        high = factor.astype(jnp.bfloat16)
        low = (factor - high.astype(jnp.float32)).astype(jnp.bfloat16)
        total = total + dot(high.T, back) + dot(low.T, back)
    moe = total[:tok_count] + swapped(total[tok_count:])
    return layer_norm(
        residual_scale * hidden_one.astype(jnp.float32) + moe, norm2_gain, norm2_bias
    ).astype(jnp.bfloat16)


def solution(mesh):
    torus = Mesh(
        mesh.devices.reshape(mesh.shape["grp"], -1, 2, mesh.shape["tp"]),
        ("grp", "sp_0", "sp_1", "tp"),
    )
    in_specs = (
        P(GRP_SP, "tp"),
        P(GRP_SP, "tp"),
        P(GRP_SP, "tp"),
        P(GRP_SP),
        P(None, "tp"),
        P("tp", None),
        P(GRP_SP_TP, None),
        P(),
        P(),
        P(GRP_SP_TP, None),
        P(GRP_SP_TP, None),
        P(SP, None, "tp"),
        P(SP, None, "tp"),
        P(SP, "tp", None),
        P(),
        P(),
    )
    out_specs = P(GRP_SP_TP, None)
    return jax.shard_map(
        shards, mesh=torus, in_specs=in_specs, out_specs=out_specs, check_vma=False
    )
```

profile of v0, /device:TPU:33, one launch (start us, length us, event | category | flops | bytes accessed | tf_op | source)
XLA Modules:
  0.0 383.8 jit_solution(6780999300419874182)
XLA Ops:
  6.6 0.8 convert_element_type.245
  7.5 1.2 convert_multiply_fusion
  8.9 5.7 %collective-permute-start = (f32[4,384]{1,0:T(4,128)S(1)}, f32[4,384]{1,0:T(4,128)S(1)}, u32[]{:S(2)}, u32[]{:S(2)}) collective-permute-start(f32[4,384]{1,0:T(4,128)S(1)} %pad_maximum_fusion.5), channel_id=1, source_target_pairs={{0,4},{4,8},{8,12},{12,16},{16,20},{20,24},{24,28},{28,32},{32,36}... | collective-permute-start | bytes 18440 | tf_op jit(solution)/shard_map/ppermute | solution.py:17
  14.6 0.7 convert_element_type.242
  15.3 15.9 %collective-permute-done = f32[4,384]{1,0:T(4,128)S(1)} collective-permute-done((f32[4,384]{1,0:T(4,128)S(1)}, f32[4,384]{1,0:T(4,128)S(1)}, u32[]{:S(2)}, u32[]{:S(2)}) %collective-permute-start) | collective-permute-done | bytes 6176 | tf_op jit(solution)/shard_map/ppermute | solution.py:17
  31.2 0.1 slice_reduce_fusion.3
  31.4 0.8 slice_compare_fusion.1
  32.2 4.4 %convolution_convert_fusion = bf16[512,2048]{1,0:T(8,128)(2,1)} fusion(bf16[384,2048]{1,0:T(8,128)(2,1)} %param.21, f32[2,384]{1,0:T(2,128)S(1)} %slice.63, f32[512,384]{1,0:T(8,128)S(1)} %convert_multiply_fusion, bf16[512,384]{1,0:T(8,128)(2,1)} %param.16, f32[384]{0:T(512)S(1)} %get-tuple-element.16, f32[384]{0:T(512)S(1)} %get-tuple-element.17, ...), kind=kOutput, calls=%fused_computation.21 | convolution fusion | flops 808910848 | bytes 4858880 | tf_op jit(solution)/shard_map/dot_general | solution.py:31
  36.6 4.7 %all-to-all-start = ((bf16[4,128,2048]{2,1,0:T(8,128)(2,1)}), bf16[4,128,2048]{2,1,0:T(8,128)(2,1)}, u32[]{:S(2)}, u32[]{:S(2)}) async-start(bf16[4,128,2048]{2,1,0:T(8,128)(2,1)} %bitcast.127), calls=%async_computation | async-start | bytes 4194304 | tf_op jit(solution)/shard_map/all_to_all | solution.py:86
  41.3 0.3 collective-permute-start.1
  41.6 1.0 collective-permute-done.1
  42.7 0.1 fusion.43
  42.8 24.7 %all-to-all-done = bf16[4,128,2048]{2,1,0:T(8,128)(2,1)} async-done(((bf16[4,128,2048]{2,1,0:T(8,128)(2,1)}), bf16[4,128,2048]{2,1,0:T(8,128)(2,1)}, u32[]{:S(2)}, u32[]{:S(2)}) %all-to-all-start) | async-done | bytes 2097184 | tf_op jit(solution)/shard_map/all_to_all | solution.py:86
  67.5 2.1 convert_reduce_fusion
  69.7 0.2 fusion.77
  69.9 0.3 multiply_reduce_fusion.1
  70.3 0.1 copy-done.13
  70.4 0.3 add_convert_fusion.1
  70.7 1.1 collective-permute-start.2
  72.1 0.7 fusion.88
  72.8 0.6 collective-permute-done.2
  73.4 0.8 copy-done.21
  74.2 0.3 convolution_convert_fusion.3
  74.5 0.8 reshape.246
  75.3 6.6 %all-to-all-start.1 = ((bf16[16,4,2048]{2,1,0:T(4,128)(2,1)}), bf16[16,4,2048]{2,1,0:T(4,128)(2,1)S(1)}, u32[]{:S(2)}, u32[]{:S(2)}) async-start(bf16[16,4,2048]{2,1,0:T(4,128)(2,1)} %reshape.246), calls=%async_computation.1 | async-start | bytes 524288 | tf_op jit(solution)/shard_map/all_to_all | solution.py:121
  81.9 0.1 broadcast_compare_fusion
  82.1 1.8 fusion.83
  83.8 2.3 fusion.31
  86.2 1.1 fusion.32
  87.3 8.4 %all-to-all-done.1 = bf16[16,4,2048]{2,1,0:T(4,128)(2,1)S(1)} async-done(((bf16[16,4,2048]{2,1,0:T(4,128)(2,1)}), bf16[16,4,2048]{2,1,0:T(4,128)(2,1)S(1)}, u32[]{:S(2)}, u32[]{:S(2)}) %all-to-all-start.1) | async-done | bytes 262176 | tf_op jit(solution)/shard_map/all_to_all | solution.py:121
  95.7 10.4 %all-to-all-start.3 = ((bf16[16,8,2048]{2,1,0:T(8,128)(2,1)}), bf16[16,8,2048]{2,1,0:T(8,128)(2,1)}, u32[]{:S(2)}, u32[]{:S(2)}) async-start(bf16[16,8,2048]{2,1,0:T(8,128)(2,1)} %fusion.31), calls=%async_computation.4 | async-start | bytes 1048576 | tf_op jit(solution)/shard_map/all_to_all | solution.py:121
  106.2 0.8 reshape.249
  107.1 21.9 %all-to-all-done.3 = bf16[16,8,2048]{2,1,0:T(8,128)(2,1)} async-done(((bf16[16,8,2048]{2,1,0:T(8,128)(2,1)}), bf16[16,8,2048]{2,1,0:T(8,128)(2,1)}, u32[]{:S(2)}, u32[]{:S(2)}) %all-to-all-start.3) | async-done | bytes 524320 | tf_op jit(solution)/shard_map/all_to_all | solution.py:121
  129.1 35.6 %all_to_all.35 = bf16[16,8,2048]{2,1,0:T(8,128)(2,1)} all-to-all(bf16[16,8,2048]{2,1,0:T(8,128)(2,1)} %fusion.32), channel_id=1, replica_groups=mesh['grp'=2,'sp_0'=16,'sp_1'=2,'tp'=4] {'sp_0'}, dimensions={0} | all-to-all | bytes 1048576 | tf_op jit(solution)/shard_map/all_to_all | solution.py:121
  164.9 4.1 %fusion.16 = f32[256,768]{1,0:T(8,128)} fusion(bf16[256,2048]{1,0:T(8,128)(2,1)} %all-gather.4.cloned.1.call-done, bf16[1,2048,768]{2,1,0:T(8,128)(2,1)} %param.27), kind=kOutput, calls=%fused_computation.17 | convolution fusion | flops 805306368 | bytes 4980736 | tf_op jit(solution)/shard_map/dot_general | solution.py:31
  169.0 5.6 %fusion.28 = bf16[256,2048]{1,0:T(8,128)(2,1)} fusion(bf16[1,768,2048]{2,1,0:T(8,128)(2,1)S(1)} %copy-done, bf16[256,2048]{1,0:T(8,128)(2,1)} %all-gather.4.cloned.1.call-done, bf16[1,2048,768]{2,1,0:T(8,128)(2,1)} %param.28, f32[256,768]{1,0:T(8,128)} %fusion.16), kind=kOutput, calls=%fused_computation.27 | convolution fusion | flops 1612316672 | bytes 9175040 | tf_op jit(solution)/shard_map/dot_general | solution.py:31
  174.7 0.2 reduce-scatter.6.cloned.1.call-start
  174.9 3.0 all-gather.6.cloned.1.call-done
  177.9 5.5 %fusion.14 = f32[512,768]{1,0:T(8,128)} fusion(bf16[512,2048]{1,0:T(8,128)(2,1)} %all-gather.6.cloned.1.call-done, bf16[1,2048,768]{2,1,0:T(8,128)(2,1)} %param.27), kind=kOutput, calls=%fused_computation.15 | convolution fusion | flops 1610612736 | bytes 6815744 | tf_op jit(solution)/shard_map/dot_general | solution.py:31
  183.3 8.2 %fusion.18 = bf16[512,2048]{1,0:T(8,128)(2,1)} fusion(bf16[1,768,2048]{2,1,0:T(8,128)(2,1)S(1)} %copy-done, f32[512,768]{1,0:T(8,128)} %fusion.14, bf16[512,2048]{1,0:T(8,128)(2,1)} %all-gather.6.cloned.1.call-done, bf16[1,2048,768]{2,1,0:T(8,128)(2,1)} %param.28), kind=kOutput, calls=%fused_computation.19 | convolution fusion | flops 3224633344 | bytes 12058624 | tf_op jit(solution)/shard_map/dot_general | solution.py:31
  191.7 24.9 %all-gather.8.cloned.1.call-done = bf16[512,2048]{1,0:T(8,128)(2,1)} async-done(((bf16[128,2048]{1,0:T(8,128)(2,1)}), bf16[512,2048]{1,0:T(8,128)(2,1)}) %all-gather.8.cloned.1.call-update) | async-done | bytes 2097168 | tf_op jit(solution)/shard_map/all_gather | solution.py:125
  216.7 5.5 %fusion.12 = f32[512,768]{1,0:T(8,128)} fusion(bf16[512,2048]{1,0:T(8,128)(2,1)} %all-gather.8.cloned.1.call-done, bf16[1,2048,768]{2,1,0:T(8,128)(2,1)} %param.27), kind=kOutput, calls=%fused_computation.13 | convolution fusion | flops 1610612736 | bytes 6815744 | tf_op jit(solution)/shard_map/dot_general | solution.py:31
  222.1 8.3 %fusion.21 = bf16[512,2048]{1,0:T(8,128)(2,1)} fusion(bf16[1,768,2048]{2,1,0:T(8,128)(2,1)S(1)} %copy-done, f32[512,768]{1,0:T(8,128)} %fusion.12, bf16[512,2048]{1,0:T(8,128)(2,1)} %all-gather.8.cloned.1.call-done, bf16[1,2048,768]{2,1,0:T(8,128)(2,1)} %param.28), kind=kOutput, calls=%fused_computation.20 | convolution fusion | flops 3224633344 | bytes 12058624 | tf_op jit(solution)/shard_map/dot_general | solution.py:31
  230.5 17.2 %reduce-scatter.4.cloned.1.call-done = bf16[64,2048]{1,0:T(8,128)(2,1)} async-done(((bf16[256,2048]{1,0:T(8,128)(2,1)}), bf16[64,2048]{1,0:T(8,128)(2,1)}) %reduce-scatter.4.cloned.1.call-update) | async-done | bytes 262160 | tf_op jit(solution)/shard_map/reduce_scatter | solution.py:132
  247.7 1.1 reshape.250
  248.7 24.5 %all_to_all.36 = bf16[16,4,2048]{2,1,0:T(4,128)(2,1)} all-to-all(bf16[16,4,2048]{2,1,0:T(4,128)(2,1)S(1)} %reshape.250), channel_id=1, replica_groups=mesh['grp'=2,'sp_0'=16,'sp_1'=2,'tp'=4] {'sp_0'}, dimensions={0} | all-to-all | bytes 524288 | tf_op jit(solution)/shard_map/all_to_all | solution.py:136
  273.3 13.8 %reduce-scatter.6.cloned.1.call-done = bf16[128,2048]{1,0:T(8,128)(2,1)} async-done(((bf16[512,2048]{1,0:T(8,128)(2,1)}), bf16[128,2048]{1,0:T(8,128)(2,1)}) %reduce-scatter.6.cloned.1.call-update) | async-done | bytes 524304 | tf_op jit(solution)/shard_map/reduce_scatter | solution.py:132
  287.0 35.0 %all_to_all.37 = bf16[16,8,2048]{2,1,0:T(8,128)(2,1)} all-to-all(bf16[16,8,2048]{2,1,0:T(8,128)(2,1)} %bitcast.130), channel_id=1, replica_groups=mesh['grp'=2,'sp_0'=16,'sp_1'=2,'tp'=4] {'sp_0'}, dimensions={0} | all-to-all | bytes 1048576 | tf_op jit(solution)/shard_map/all_to_all | solution.py:136
  322.0 3.0 reduce-scatter.8.cloned.1.call-done
  325.0 12.1 %all-to-all-start.6 = ((bf16[16,8,2048]{2,1,0:T(8,128)(2,1)}), bf16[16,8,2048]{2,1,0:T(8,128)(2,1)}, u32[]{:S(2)}, u32[]{:S(2)}) async-start(bf16[16,8,2048]{2,1,0:T(8,128)(2,1)} %bitcast.129), calls=%async_computation.9 | async-start | bytes 1048576 | tf_op jit(solution)/shard_map/all_to_all | solution.py:136
  337.2 0.7 fusion.87
  337.9 1.0 reshape.251
  338.9 2.6 fusion.109
  341.5 1.8 fusion.64
  343.3 1.8 fusion.66
  345.1 14.9 %all-to-all-done.6 = bf16[16,8,2048]{2,1,0:T(8,128)(2,1)} async-done(((bf16[16,8,2048]{2,1,0:T(8,128)(2,1)}), bf16[16,8,2048]{2,1,0:T(8,128)(2,1)}, u32[]{:S(2)}, u32[]{:S(2)}) %all-to-all-start.6) | async-done | bytes 524320 | tf_op jit(solution)/shard_map/all_to_all | solution.py:136
  360.0 1.6 fusion.60
  361.7 1.5 fusion.62
  363.2 2.5 fusion.27
  365.8 7.2 %collective-permute-start.3 = (f32[128,2048]{1,0:T(8,128)S(1)}, f32[128,2048]{1,0:T(8,128)S(1)}, u32[]{:S(2)}, u32[]{:S(2)}) collective-permute-start(f32[128,2048]{1,0:T(8,128)S(1)} %slice.71), channel_id=1, source_target_pairs={{0,4},{4,0},{1,5},{5,1},{2,6},{6,2},{3,7},{7,3},{8,12},{12,8},{9,1... | collective-permute-start | bytes 3145736 | tf_op jit(solution)/shard_map/ppermute | solution.py:21
  373.0 2.3 collective-permute-done.3
  375.3 0.3 fusion.122
  375.6 0.3 multiply_reduce_fusion
  375.9 1.0 add_convert_fusion
  (80 shorter events, 1.5 us)
Async XLA Ops:
  6.5 162.5 %copy-start = (bf16[1,768,2048]{2,1,0:T(8,128)(2,1)S(1)}, bf16[1,768,2048]{2,1,0:T(8,128)(2,1)}, u32[]{:S(2)}) copy-start(bf16[1,768,2048]{2,1,0:T(8,128)(2,1)} %param.29) | copy-start | bytes 9437188
  8.9 22.4 %collective-permute-start = (f32[4,384]{1,0:T(4,128)S(1)}, f32[4,384]{1,0:T(4,128)S(1)}, u32[]{:S(2)}, u32[]{:S(2)}) collective-permute-start(f32[4,384]{1,0:T(4,128)S(1)} %pad_maximum_fusion.5), channel_id=1, source_target_pairs={{0,4},{4,8},{8,12},{12,16},{16,20},{20,24},{24,28},{28,32},{32,36}... | collective-permute-start | bytes 18440 | tf_op jit(solution)/shard_map/ppermute | solution.py:17
  36.6 4.7 %copy-start.19 = (s32[128,2]{0,1:T(2,128)S(1)}, s32[128,2]{0,1:T(2,128)}, u32[]{:S(2)}) copy-start(s32[128,2]{0,1:T(2,128)} %param.25) | copy-start | bytes 3076
  36.6 4.7 %copy-start.20 = (f32[128,2]{0,1:T(2,128)S(1)}, f32[128,2]{0,1:T(2,128)}, u32[]{:S(2)}) copy-start(f32[128,2]{0,1:T(2,128)} %param.26) | copy-start | bytes 3076
  36.6 30.9 %all-to-all-start = ((bf16[4,128,2048]{2,1,0:T(8,128)(2,1)}), bf16[4,128,2048]{2,1,0:T(8,128)(2,1)}, u32[]{:S(2)}, u32[]{:S(2)}) async-start(bf16[4,128,2048]{2,1,0:T(8,128)(2,1)} %bitcast.127), calls=%async_computation | async-start | bytes 4194304 | tf_op jit(solution)/shard_map/all_to_all | solution.py:86
  41.3 1.3 collective-permute-start.1
  41.6 30.5 %copy-start.17 = (pred[2,2]{1,0:T(4,128)(4,1)}, pred[2,2]{1,0:T(4,128)(4,1)S(1)}, u32[]{:S(2)}) copy-start(pred[2,2]{1,0:T(4,128)(4,1)S(1)} %iota_compare_fusion.1) | copy-start | bytes 16
  67.5 2.2 copy-start.3
  69.7 0.7 copy-start.13
  69.7 0.7 copy-start.14
  70.7 2.7 copy-start.5
  70.7 2.7 collective-permute-start.2
  72.1 1.3 copy-start.10
  73.4 0.8 copy-start.21
  75.3 20.4 %all-to-all-start.1 = ((bf16[16,4,2048]{2,1,0:T(4,128)(2,1)}), bf16[16,4,2048]{2,1,0:T(4,128)(2,1)S(1)}, u32[]{:S(2)}, u32[]{:S(2)}) async-start(bf16[16,4,2048]{2,1,0:T(4,128)(2,1)} %reshape.246), calls=%async_computation.1 | async-start | bytes 524288 | tf_op jit(solution)/shard_map/all_to_all | solution.py:121
  81.9 4.3 %copy-start.6 = (bf16[128,2048]{1,0:T(8,128)(2,1)S(1)}, bf16[128,2048]{1,0:T(8,128)(2,1)}, u32[]{:S(2)}) copy-start(bf16[128,2048]{1,0:T(8,128)(2,1)} %copy-done.5) | copy-start | bytes 1572868
  81.9 4.2 %copy-start.22 = (bf16[128,2048]{1,0:T(8,128)(2,1)S(1)}, bf16[128,2048]{1,0:T(8,128)(2,1)}, u32[]{:S(2)}) copy-start(bf16[128,2048]{1,0:T(8,128)(2,1)} %copy-done.21) | copy-start | bytes 1572868
  95.7 33.3 %all-to-all-start.3 = ((bf16[16,8,2048]{2,1,0:T(8,128)(2,1)}), bf16[16,8,2048]{2,1,0:T(8,128)(2,1)}, u32[]{:S(2)}, u32[]{:S(2)}) async-start(bf16[16,8,2048]{2,1,0:T(8,128)(2,1)} %fusion.31), calls=%async_computation.4 | async-start | bytes 1048576 | tf_op jit(solution)/shard_map/all_to_all | solution.py:121
  106.2 58.7 %all-gather.4.cloned.1.call-start = ((), (), s32[]{:S(2)}) async-start(), calls=%async_computation.10 | async-start | bytes 1310720 | tf_op jit(solution)/shard_map/all_gather | solution.py:125
  107.1 70.8 %all-gather.6.cloned.1.call-start = ((), (), s32[]{:S(2)}) async-start(), calls=%async_computation.12 | async-start | bytes 2621440 | tf_op jit(solution)/shard_map/all_gather | solution.py:125
  129.1 87.6 %all-gather.8.cloned.1.call-start = ((), (), s32[]{:S(2)}) async-start(), calls=%async_computation.14 | async-start | bytes 2621440 | tf_op jit(solution)/shard_map/all_gather | solution.py:125
  164.8 82.9 %reduce-scatter.4.cloned.1.call-start = ((), (), s32[]{:S(2)}) async-start(), calls=%async_computation.11 | async-start | bytes 1310720 | tf_op jit(solution)/shard_map/reduce_scatter | solution.py:132
  174.7 112.3 %reduce-scatter.6.cloned.1.call-start = ((), (), s32[]{:S(2)}) async-start(), calls=%async_computation.13 | async-start | bytes 2621440 | tf_op jit(solution)/shard_map/reduce_scatter | solution.py:132
  191.7 133.4 %reduce-scatter.8.cloned.1.call-start = ((), (), s32[]{:S(2)}) async-start(), calls=%async_computation.15 | async-start | bytes 2621440 | tf_op jit(solution)/shard_map/reduce_scatter | solution.py:132
  273.3 63.9 %copy-start.11 = (pred[16,2,2,128]{3,2,1,0:T(4,128)(4,1)S(1)}, pred[16,2,2,128]{3,2,1,0:T(4,128)(4,1)}, u32[]{:S(2)}) copy-start(pred[16,2,2,128]{3,2,1,0:T(4,128)(4,1)} %copy-done.10) | copy-start | bytes 24580
  273.3 63.9 %copy-start.18 = (pred[2,2]{1,0:T(4,128)(4,1)S(1)}, pred[2,2]{1,0:T(4,128)(4,1)}, u32[]{:S(2)}) copy-start(pred[2,2]{1,0:T(4,128)(4,1)} %copy-done.17) | copy-start | bytes 16
  325.0 35.0 %all-to-all-start.6 = ((bf16[16,8,2048]{2,1,0:T(8,128)(2,1)}), bf16[16,8,2048]{2,1,0:T(8,128)(2,1)}, u32[]{:S(2)}, u32[]{:S(2)}) async-start(bf16[16,8,2048]{2,1,0:T(8,128)(2,1)} %bitcast.129), calls=%async_computation.9 | async-start | bytes 1048576 | tf_op jit(solution)/shard_map/all_to_all | solution.py:136
  338.9 2.6 copy-start.4
  338.9 2.6 copy-start.9
  338.9 4.4 %copy-start.8 = (bf16[16,2,4,2,128]{4,3,2,1,0:T(2,128)(2,1)S(1)}, bf16[16,2,4,2,128]{4,3,2,1,0:T(2,128)(2,1)}, u32[]{:S(2)}) copy-start(bf16[16,2,4,2,128]{4,3,2,1,0:T(2,128)(2,1)} %get-tuple-element.21) | copy-start | bytes 196612
  360.0 3.1 copy-start.1
  360.0 3.2 copy-start.2
  360.0 3.2 copy-start.12
  365.7 9.6 %copy-start.7 = (bf16[128,2048]{1,0:T(8,128)(2,1)S(1)}, bf16[128,2048]{1,0:T(8,128)(2,1)}, u32[]{:S(2)}) copy-start(bf16[128,2048]{1,0:T(8,128)(2,1)} %copy-done.5) | copy-start | bytes 1572868
  365.8 10.1 %copy-start.15 = (f32[2048]{0:T(1024)S(1)}, f32[2048]{0:T(1024)}, u32[]{:S(2)}) copy-start(f32[2048]{0:T(1024)} %param.31) | copy-start | bytes 24580
  365.8 10.1 %copy-start.16 = (f32[2048]{0:T(1024)S(1)}, f32[2048]{0:T(1024)}, u32[]{:S(2)}) copy-start(f32[2048]{0:T(1024)} %param.30) | copy-start | bytes 24580
  365.8 9.4 %collective-permute-start.3 = (f32[128,2048]{1,0:T(8,128)S(1)}, f32[128,2048]{1,0:T(8,128)S(1)}, u32[]{:S(2)}, u32[]{:S(2)}) collective-permute-start(f32[128,2048]{1,0:T(8,128)S(1)} %slice.71), channel_id=1, source_target_pairs={{0,4},{4,0},{1,5},{5,1},{2,6},{6,2},{3,7},{7,3},{8,12},{12,8},{9,1... | collective-permute-start | bytes 3145736 | tf_op jit(solution)/shard_map/ppermute | solution.py:21
Sparse Core Ops, SparseCore 0:
  108.8 27.9 all-gather.3
  138.7 39.1 all-gather.5
  179.7 36.8 all-gather.7
  219.1 28.5 reduce-scatter.3
  250.1 36.8 reduce-scatter.5
  289.4 35.5 reduce-scatter.7
where the time goes:
time: 385 us; the launch traced here: 384 us
  waiting for transfers between devices  152 us (39%)
  blocking collectives  95.1 us (25%)
  matrix products  57.3 us (15%)
  starting transfers between devices  48.7 us (13%)
  between operations  13.9 us (4%)
  other arithmetic  11.9 us (3%)
  local copies, waits for them, and re-layouts  5.08 us (1%)
    all_to_all x2, blocking collectives, shards(): back = lax.all_to_all(ready, 'sp_0', 0, 0, tiled=True).reshape(-1, width)  59.5 us
    dot_general x17, matrix products, dot(): return jnp.dot(a, b, preferred_element_type=jnp.float32)  57.3 us
    all_to_all x1, blocking collectives, shards(): moved = lax.all_to_all(packed[i], 'sp_0', 0, 0, tiled=True)  35.6 us
    reduce_scatter x3, waiting for transfers between devices, shards(): lax.psum_scatter(piece, 'tp', scatter_dimension=0, tiled=True)  34 us
    all_to_all x2, waiting for transfers between devices, shards(): moved = lax.all_to_all(packed[i], 'sp_0', 0, 0, tiled=True)  30.3 us
    all_gather x3, waiting for transfers between devices, shards(): lax.all_gather(moved.reshape(-1, width), 'tp', axis=0, tiled=True)  27.9 us
    all_to_all x1, waiting for transfers between devices, shards(): lax.all_to_all(partial.reshape(n_tp, row_count // n_tp, width), 'tp', 0,...  24.7 us
    all_to_all x2, starting transfers between devices, shards(): moved = lax.all_to_all(packed[i], 'sp_0', 0, 0, tiled=True)  17 us
  transfers between devices with their start and end apart: 14, of which 13 were waited for; matrix products, arithmetic and copies ran while one was open for 14% of the time, Pallas kernels for 0%

commit v1 on v0

--- a/solution.py
+++ b/solution.py
@@ -10,6 +10,12 @@
 SUBLANES = 8
 residual_scale = 2.0**0.5
 norm_eps = 1e-05
+
+
+def drive_view(w_in):
+    everything = tuple((w_in for _ in range(lax.axis_size("tp"))))
+    extra = jnp.concatenate(everything, axis=0)
+    return lax.all_to_all(extra, "tp", 0, 0, tiled=True)
 
 
 def next_in_sequence(x):
@@ -122,7 +128,7 @@
         rest = tuple(packed[i + 1 :])
         moved, rest = lax.optimization_barrier((moved, rest))
         packed[i + 1 :] = list(rest)
-        gathered.append(lax.all_gather(moved.reshape(-1, width), "tp", axis=0, tiled=True))
+        gathered.append(drive_view(moved.reshape(-1, width)))
     scattered = []
     for rows_in in gathered:
         gate_act = dot(rows_in, w_gate[0])

time: 385 us -> 394 us (1.023)
  starting transfers between devices: 48.7 us -> 94.1 us
  blocking collectives: 95.1 us -> 71.2 us
  waiting for transfers between devices: 152 us -> 131 us
  other arithmetic: 11.9 us -> 18.2 us
    reduce_scatter x3, waiting for transfers between devices: 34 us -> 0.04 us  [shards(): lax.psum_scatter(piece, 'tp', scatter_dimension=0, tiled=True)]
    all_gather x3 -> x0, waiting for transfers between devices: 27.9 us -> none  [shards(): lax.all_gather(moved.reshape(-1, width), 'tp', axis=0, tiled=True)]
    all_to_all x2 -> x1, blocking collectives: 59.5 us -> 32.3 us  [shards(): back = lax.all_to_all(ready, 'sp_0', 0, 0, tiled=True).reshape(-1, width)]
    all_to_all x2 -> x3, starting transfers between devices: 17 us -> 41.6 us  [shards(): moved = lax.all_to_all(packed[i], 'sp_0', 0, 0, tiled=True)]
    all_to_all x1 -> x2, waiting for transfers between devices: 14.9 us -> 35.8 us  [shards(): back = lax.all_to_all(ready, 'sp_0', 0, 0, tiled=True).reshape(-1, width)]
    all_to_all x0 -> x2, waiting for transfers between devices: none -> 14.7 us  [drive_view(): return lax.all_to_all(extra, 'tp', 0, 0, tiled=True)]
    all_to_all x1 -> x2, starting transfers between devices: 12.1 us -> 24.2 us  [shards(): back = lax.all_to_all(ready, 'sp_0', 0, 0, tiled=True).reshape(-1, width)]
    all_to_all x0 -> x2, starting transfers between devices: none -> 8.88 us  [drive_view(): return lax.all_to_all(extra, 'tp', 0, 0, tiled=True)]
  transfers between devices with their start and end apart: 14 -> 15, of which waited for: 13 -> 12; matrix products, arithmetic and copies ran while one was open for 14% -> 15% of each run, Pallas kernels for 0% -> 0%
where the time goes in v1:
time: 394 us; the launch traced here: 393 us
  waiting for transfers between devices  131 us (33%)
  starting transfers between devices  94.1 us (24%)
  blocking collectives  71.2 us (18%)
  matrix products  56.8 us (14%)
  other arithmetic  18.2 us (5%)
  between operations  13.6 us (3%)
  local copies, waits for them, and re-layouts  7.36 us (2%)
    dot_general x17, matrix products, dot(): return jnp.dot(a, b, preferred_element_type=jnp.float32)  56.8 us
    all_to_all x3, starting transfers between devices, shards(): moved = lax.all_to_all(packed[i], 'sp_0', 0, 0, tiled=True)  41.6 us
    all_to_all x1, blocking collectives, drive_view(): return lax.all_to_all(extra, 'tp', 0, 0, tiled=True)  39 us
    all_to_all x3, waiting for transfers between devices, shards(): moved = lax.all_to_all(packed[i], 'sp_0', 0, 0, tiled=True)  36.3 us
    all_to_all x2, waiting for transfers between devices, shards(): back = lax.all_to_all(ready, 'sp_0', 0, 0, tiled=True).reshape(-1, width)  35.8 us
    all_to_all x1, blocking collectives, shards(): back = lax.all_to_all(ready, 'sp_0', 0, 0, tiled=True).reshape(-1, width)  32.3 us
    all_to_all x1, waiting for transfers between devices, shards(): lax.all_to_all(partial.reshape(n_tp, row_count // n_tp, width), 'tp', 0,...  24.7 us
    all_to_all x2, starting transfers between devices, shards(): back = lax.all_to_all(ready, 'sp_0', 0, 0, tiled=True).reshape(-1, width)  24.2 us
  transfers between devices with their start and end apart: 15, of which 12 were waited for; matrix products, arithmetic and copies ran while one was open for 15% of the time, Pallas kernels for 0%

profile of v1, /device:TPU:33, one launch (start us, length us, event | category | flops | bytes accessed | tf_op | source)
XLA Modules:
  0.0 392.7 jit_solution(10408820525371587345)
XLA Ops:
  6.6 0.8 convert_element_type.245
  7.5 1.2 convert_multiply_fusion
  8.9 5.7 %collective-permute-start = (f32[4,384]{1,0:T(4,128)S(1)}, f32[4,384]{1,0:T(4,128)S(1)}, u32[]{:S(2)}, u32[]{:S(2)}) collective-permute-start(f32[4,384]{1,0:T(4,128)S(1)} %pad_maximum_fusion.8), channel_id=1, source_target_pairs={{0,4},{4,8},{8,12},{12,16},{16,20},{20,24},{24,28},{28,32},{32,36}... | collective-permute-start | bytes 18440 | tf_op jit(solution)/shard_map/ppermute | solution.py:23
  14.6 0.7 convert_element_type.242
  15.3 15.9 %collective-permute-done = f32[4,384]{1,0:T(4,128)S(1)} collective-permute-done((f32[4,384]{1,0:T(4,128)S(1)}, f32[4,384]{1,0:T(4,128)S(1)}, u32[]{:S(2)}, u32[]{:S(2)}) %collective-permute-start) | collective-permute-done | bytes 6176 | tf_op jit(solution)/shard_map/ppermute | solution.py:23
  31.4 0.8 slice_compare_fusion.1
  32.2 4.4 %convolution_convert_fusion = bf16[512,2048]{1,0:T(8,128)(2,1)} fusion(bf16[384,2048]{1,0:T(8,128)(2,1)} %param.21, f32[2,384]{1,0:T(2,128)S(1)} %slice.63, f32[512,384]{1,0:T(8,128)S(1)} %convert_multiply_fusion, bf16[512,384]{1,0:T(8,128)(2,1)} %param.16, f32[384]{0:T(512)S(1)} %get-tuple-element.16, f32[384]{0:T(512)S(1)} %get-tuple-element.17, ...), kind=kOutput, calls=%fused_computation.21 | convolution fusion | flops 808910848 | bytes 4858880 | tf_op jit(solution)/shard_map/dot_general | solution.py:37
  36.6 4.7 %all-to-all-start = ((bf16[4,128,2048]{2,1,0:T(8,128)(2,1)}), bf16[4,128,2048]{2,1,0:T(8,128)(2,1)}, u32[]{:S(2)}, u32[]{:S(2)}) async-start(bf16[4,128,2048]{2,1,0:T(8,128)(2,1)} %bitcast.136), calls=%async_computation | async-start | bytes 4194304 | tf_op jit(solution)/shard_map/all_to_all | solution.py:92
  41.3 0.3 collective-permute-start.1
  41.6 1.0 collective-permute-done.1
  42.8 24.7 %all-to-all-done = bf16[4,128,2048]{2,1,0:T(8,128)(2,1)} async-done(((bf16[4,128,2048]{2,1,0:T(8,128)(2,1)}), bf16[4,128,2048]{2,1,0:T(8,128)(2,1)}, u32[]{:S(2)}, u32[]{:S(2)}) %all-to-all-start) | async-done | bytes 2097184 | tf_op jit(solution)/shard_map/all_to_all | solution.py:92
  67.5 2.1 convert_reduce_fusion
  70.0 0.3 multiply_reduce_fusion.1
  70.4 0.3 add_convert_fusion.1
  70.7 1.1 collective-permute-start.2
  72.1 0.7 fusion.88
  72.8 0.6 collective-permute-done.2
  73.4 0.8 copy-done.23
  74.2 0.3 convolution_convert_fusion.3
  74.5 0.8 reshape.252
  75.3 6.6 %all-to-all-start.1 = ((bf16[16,4,2048]{2,1,0:T(4,128)(2,1)}), bf16[16,4,2048]{2,1,0:T(4,128)(2,1)S(1)}, u32[]{:S(2)}, u32[]{:S(2)}) async-start(bf16[16,4,2048]{2,1,0:T(4,128)(2,1)} %reshape.252), calls=%async_computation.1 | async-start | bytes 524288 | tf_op jit(solution)/shard_map/all_to_all | solution.py:127
  82.0 1.8 fusion.83
  83.8 2.3 fusion.31
  86.1 1.1 fusion.32
  87.2 8.4 %all-to-all-done.1 = bf16[16,4,2048]{2,1,0:T(4,128)(2,1)S(1)} async-done(((bf16[16,4,2048]{2,1,0:T(4,128)(2,1)}), bf16[16,4,2048]{2,1,0:T(4,128)(2,1)S(1)}, u32[]{:S(2)}, u32[]{:S(2)}) %all-to-all-start.1) | async-done | bytes 262176 | tf_op jit(solution)/shard_map/all_to_all | solution.py:127
  95.7 0.7 copy-done.8
  96.4 10.4 %all-to-all-start.4 = ((bf16[16,8,2048]{2,1,0:T(8,128)(2,1)}), bf16[16,8,2048]{2,1,0:T(8,128)(2,1)}, u32[]{:S(2)}, u32[]{:S(2)}) async-start(bf16[16,8,2048]{2,1,0:T(8,128)(2,1)} %fusion.31), calls=%async_computation.5 | async-start | bytes 1048576 | tf_op jit(solution)/shard_map/all_to_all | solution.py:127
  106.8 1.0 reshape.255
  107.8 1.1 pad_maximum_fusion.3
  108.9 20.7 %all-to-all-done.4 = bf16[16,8,2048]{2,1,0:T(8,128)(2,1)} async-done(((bf16[16,8,2048]{2,1,0:T(8,128)(2,1)}), bf16[16,8,2048]{2,1,0:T(8,128)(2,1)}, u32[]{:S(2)}, u32[]{:S(2)}) %all-to-all-start.4) | async-done | bytes 524320 | tf_op jit(solution)/shard_map/all_to_all | solution.py:127
  129.7 4.3 %all-to-all-start.2 = ((bf16[4,64,2048]{2,1,0:T(8,128)(2,1)}), bf16[4,64,2048]{2,1,0:T(8,128)(2,1)}, u32[]{:S(2)}, u32[]{:S(2)}) async-start(bf16[4,64,2048]{2,1,0:T(8,128)(2,1)} %bitcast.135), calls=%async_computation.2 | async-start | bytes 2097152 | tf_op jit(solution)/shard_map/all_to_all | solution.py:18
  134.0 3.3 pad_maximum_fusion
  137.3 6.5 %all-to-all-done.2 = bf16[4,64,2048]{2,1,0:T(8,128)(2,1)} async-done(((bf16[4,64,2048]{2,1,0:T(8,128)(2,1)}), bf16[4,64,2048]{2,1,0:T(8,128)(2,1)}, u32[]{:S(2)}, u32[]{:S(2)}) %all-to-all-start.2) | async-done | bytes 1048608 | tf_op jit(solution)/shard_map/all_to_all | solution.py:18
  143.8 4.5 %all-to-all-start.5 = ((bf16[4,128,2048]{2,1,0:T(8,128)(2,1)}), bf16[4,128,2048]{2,1,0:T(8,128)(2,1)}, u32[]{:S(2)}, u32[]{:S(2)}) async-start(bf16[4,128,2048]{2,1,0:T(8,128)(2,1)} %bitcast.133), calls=%async_computation.6 | async-start | bytes 4194304 | tf_op jit(solution)/shard_map/all_to_all | solution.py:18
  148.4 4.1 %fusion.16 = f32[256,768]{1,0:T(8,128)} fusion(bf16[256,2048]{1,0:T(8,128)(2,1)} %bitcast.11, bf16[1,2048,768]{2,1,0:T(8,128)(2,1)} %param.27), kind=kOutput, calls=%fused_computation.17 | convolution fusion | flops 805306368 | bytes 4980736 | tf_op jit(solution)/shard_map/dot_general | solution.py:37
  152.5 5.5 %fusion.28 = bf16[256,2048]{1,0:T(8,128)(2,1)} fusion(bf16[1,768,2048]{2,1,0:T(8,128)(2,1)S(1)} %copy-done, bf16[256,2048]{1,0:T(8,128)(2,1)} %bitcast.11, bf16[1,2048,768]{2,1,0:T(8,128)(2,1)} %param.28, f32[256,768]{1,0:T(8,128)} %fusion.16), kind=kOutput, calls=%fused_computation.27 | convolution fusion | flops 1612316672 | bytes 9175040 | tf_op jit(solution)/shard_map/dot_general | solution.py:37
  158.1 8.2 %all-to-all-done.5 = bf16[4,128,2048]{2,1,0:T(8,128)(2,1)} async-done(((bf16[4,128,2048]{2,1,0:T(8,128)(2,1)}), bf16[4,128,2048]{2,1,0:T(8,128)(2,1)}, u32[]{:S(2)}, u32[]{:S(2)}) %all-to-all-start.5) | async-done | bytes 2097184 | tf_op jit(solution)/shard_map/all_to_all | solution.py:18
  166.3 24.6 %all-to-all-start.7 = ((bf16[16,8,2048]{2,1,0:T(8,128)(2,1)}), bf16[16,8,2048]{2,1,0:T(8,128)(2,1)}, u32[]{:S(2)}, u32[]{:S(2)}) async-start(bf16[16,8,2048]{2,1,0:T(8,128)(2,1)} %fusion.32), calls=%async_computation.9 | async-start | bytes 1048576 | tf_op jit(solution)/shard_map/all_to_all | solution.py:127
  191.2 5.6 %fusion.14 = f32[512,768]{1,0:T(8,128)} fusion(bf16[512,2048]{1,0:T(8,128)(2,1)} %bitcast.17, bf16[1,2048,768]{2,1,0:T(8,128)(2,1)} %param.27), kind=kOutput, calls=%fused_computation.15 | convolution fusion | flops 1610612736 | bytes 6815744 | tf_op jit(solution)/shard_map/dot_general | solution.py:37
  196.7 8.3 %fusion.18 = bf16[512,2048]{1,0:T(8,128)(2,1)} fusion(bf16[1,768,2048]{2,1,0:T(8,128)(2,1)S(1)} %copy-done, f32[512,768]{1,0:T(8,128)} %fusion.14, bf16[512,2048]{1,0:T(8,128)(2,1)} %bitcast.17, bf16[1,2048,768]{2,1,0:T(8,128)(2,1)} %param.28), kind=kOutput, calls=%fused_computation.19 | convolution fusion | flops 3224633344 | bytes 12058624 | tf_op jit(solution)/shard_map/dot_general | solution.py:37
  205.1 7.2 %all-to-all-done.7 = bf16[16,8,2048]{2,1,0:T(8,128)(2,1)} async-done(((bf16[16,8,2048]{2,1,0:T(8,128)(2,1)}), bf16[16,8,2048]{2,1,0:T(8,128)(2,1)}, u32[]{:S(2)}, u32[]{:S(2)}) %all-to-all-start.7) | async-done | bytes 524320 | tf_op jit(solution)/shard_map/all_to_all | solution.py:127
  212.3 2.0 pad_maximum_fusion.1
  214.3 39.0 %all_to_all.71 = bf16[4,128,2048]{2,1,0:T(8,128)(2,1)S(1)} all-to-all(bf16[4,128,2048]{2,1,0:T(8,128)(2,1)S(1)} %bitcast.134), channel_id=1, replica_groups=mesh['grp'=2,'sp_0'=16,'sp_1'=2,'tp'=4] {'tp'}, dimensions={0} | all-to-all | bytes 4194304 | tf_op jit(solution)/shard_map/all_to_all | solution.py:18
  253.3 1.3 copy-done.4
  254.6 2.9 fusion.12
  257.6 8.3 %fusion.21 = bf16[512,2048]{1,0:T(8,128)(2,1)} fusion(bf16[1,768,2048]{2,1,0:T(8,128)(2,1)S(1)} %copy-done, f32[512,768]{1,0:T(8,128)} %fusion.12, bf16[512,2048]{1,0:T(8,128)(2,1)} %bitcast.138, bf16[1,2048,768]{2,1,0:T(8,128)(2,1)} %param.28), kind=kOutput, calls=%fused_computation.20 | convolution fusion | flops 3224633344 | bytes 12058624 | tf_op jit(solution)/shard_map/dot_general | solution.py:37
  265.9 1.1 reshape.256
  267.0 32.3 %all_to_all.72 = bf16[16,4,2048]{2,1,0:T(4,128)(2,1)} all-to-all(bf16[16,4,2048]{2,1,0:T(4,128)(2,1)S(1)} %reshape.256), channel_id=1, replica_groups=mesh['grp'=2,'sp_0'=16,'sp_1'=2,'tp'=4] {'sp_0'}, dimensions={0} | all-to-all | bytes 524288 | tf_op jit(solution)/shard_map/all_to_all | solution.py:142
  299.2 11.7 %all-to-all-start.6 = ((bf16[16,8,2048]{2,1,0:T(8,128)(2,1)}), bf16[16,8,2048]{2,1,0:T(8,128)(2,1)}, u32[]{:S(2)}, u32[]{:S(2)}) async-start(bf16[16,8,2048]{2,1,0:T(8,128)(2,1)} %bitcast.139), calls=%async_computation.8 | async-start | bytes 1048576 | tf_op jit(solution)/shard_map/all_to_all | solution.py:142
  311.0 22.9 %all-to-all-done.6 = bf16[16,8,2048]{2,1,0:T(8,128)(2,1)} async-done(((bf16[16,8,2048]{2,1,0:T(8,128)(2,1)}), bf16[16,8,2048]{2,1,0:T(8,128)(2,1)}, u32[]{:S(2)}, u32[]{:S(2)}) %all-to-all-start.6) | async-done | bytes 524320 | tf_op jit(solution)/shard_map/all_to_all | solution.py:142
  333.9 12.5 %all-to-all-start.9 = ((bf16[16,8,2048]{2,1,0:T(8,128)(2,1)}), bf16[16,8,2048]{2,1,0:T(8,128)(2,1)}, u32[]{:S(2)}, u32[]{:S(2)}) async-start(bf16[16,8,2048]{2,1,0:T(8,128)(2,1)} %bitcast.140), calls=%async_computation.12 | async-start | bytes 1048576 | tf_op jit(solution)/shard_map/all_to_all | solution.py:142
  346.4 0.7 fusion.87
  347.1 1.0 reshape.257
  348.2 2.6 fusion.109
  350.8 2.8 fusion.64
  353.6 2.8 fusion.66
  356.4 12.9 %all-to-all-done.9 = bf16[16,8,2048]{2,1,0:T(8,128)(2,1)} async-done(((bf16[16,8,2048]{2,1,0:T(8,128)(2,1)}), bf16[16,8,2048]{2,1,0:T(8,128)(2,1)}, u32[]{:S(2)}, u32[]{:S(2)}) %all-to-all-start.9) | async-done | bytes 524320 | tf_op jit(solution)/shard_map/all_to_all | solution.py:142
  369.3 1.6 fusion.60
  371.0 1.5 fusion.62
  372.5 2.5 fusion.27
  375.1 7.2 %collective-permute-start.3 = (f32[128,2048]{1,0:T(8,128)S(1)}, f32[128,2048]{1,0:T(8,128)S(1)}, u32[]{:S(2)}, u32[]{:S(2)}) collective-permute-start(f32[128,2048]{1,0:T(8,128)S(1)} %slice.71), channel_id=1, source_target_pairs={{0,4},{4,0},{1,5},{5,1},{2,6},{6,2},{3,7},{7,3},{8,12},{12,8},{9,1... | collective-permute-start | bytes 3145736 | tf_op jit(solution)/shard_map/ppermute | solution.py:27
  382.3 2.3 collective-permute-done.3
  384.6 0.3 fusion.122
  385.2 1.0 add_convert_fusion
  (85 shorter events, 2.4 us)
Async XLA Ops:
  6.5 145.9 %copy-start = (bf16[1,768,2048]{2,1,0:T(8,128)(2,1)S(1)}, bf16[1,768,2048]{2,1,0:T(8,128)(2,1)}, u32[]{:S(2)}) copy-start(bf16[1,768,2048]{2,1,0:T(8,128)(2,1)} %param.29) | copy-start | bytes 9437188
  8.9 22.4 %collective-permute-start = (f32[4,384]{1,0:T(4,128)S(1)}, f32[4,384]{1,0:T(4,128)S(1)}, u32[]{:S(2)}, u32[]{:S(2)}) collective-permute-start(f32[4,384]{1,0:T(4,128)S(1)} %pad_maximum_fusion.8), channel_id=1, source_target_pairs={{0,4},{4,8},{8,12},{12,16},{16,20},{20,24},{24,28},{28,32},{32,36}... | collective-permute-start | bytes 18440 | tf_op jit(solution)/shard_map/ppermute | solution.py:23
  36.6 4.7 %copy-start.20 = (s32[128,2]{0,1:T(2,128)S(1)}, s32[128,2]{0,1:T(2,128)}, u32[]{:S(2)}) copy-start(s32[128,2]{0,1:T(2,128)} %param.25) | copy-start | bytes 3076
  36.6 4.7 %copy-start.21 = (f32[128,2]{0,1:T(2,128)S(1)}, f32[128,2]{0,1:T(2,128)}, u32[]{:S(2)}) copy-start(f32[128,2]{0,1:T(2,128)} %param.26) | copy-start | bytes 3076
  36.6 30.9 %all-to-all-start = ((bf16[4,128,2048]{2,1,0:T(8,128)(2,1)}), bf16[4,128,2048]{2,1,0:T(8,128)(2,1)}, u32[]{:S(2)}, u32[]{:S(2)}) async-start(bf16[4,128,2048]{2,1,0:T(8,128)(2,1)} %bitcast.136), calls=%async_computation | async-start | bytes 4194304 | tf_op jit(solution)/shard_map/all_to_all | solution.py:92
  41.3 1.3 collective-permute-start.1
  41.6 30.5 %copy-start.18 = (pred[2,2]{1,0:T(4,128)(4,1)}, pred[2,2]{1,0:T(4,128)(4,1)S(1)}, u32[]{:S(2)}) copy-start(pred[2,2]{1,0:T(4,128)(4,1)S(1)} %iota_compare_fusion.1) | copy-start | bytes 16
  67.5 2.2 copy-start.3
  69.7 0.7 copy-start.14
  69.7 0.7 copy-start.15
  70.7 2.7 copy-start.5
  70.7 2.7 collective-permute-start.2
  72.1 1.3 copy-start.11
  73.4 0.8 copy-start.23
  75.3 20.4 %all-to-all-start.1 = ((bf16[16,4,2048]{2,1,0:T(4,128)(2,1)}), bf16[16,4,2048]{2,1,0:T(4,128)(2,1)S(1)}, u32[]{:S(2)}, u32[]{:S(2)}) async-start(bf16[16,4,2048]{2,1,0:T(4,128)(2,1)} %reshape.252), calls=%async_computation.1 | async-start | bytes 524288 | tf_op jit(solution)/shard_map/all_to_all | solution.py:127
  81.9 4.3 %copy-start.6 = (bf16[128,2048]{1,0:T(8,128)(2,1)S(1)}, bf16[128,2048]{1,0:T(8,128)(2,1)}, u32[]{:S(2)}) copy-start(bf16[128,2048]{1,0:T(8,128)(2,1)} %copy-done.5) | copy-start | bytes 1572868
  81.9 4.3 %copy-start.24 = (bf16[128,2048]{1,0:T(8,128)(2,1)S(1)}, bf16[128,2048]{1,0:T(8,128)(2,1)}, u32[]{:S(2)}) copy-start(bf16[128,2048]{1,0:T(8,128)(2,1)} %copy-done.23) | copy-start | bytes 1572868
  95.7 0.7 copy-start.8
  96.4 33.3 %all-to-all-start.4 = ((bf16[16,8,2048]{2,1,0:T(8,128)(2,1)}), bf16[16,8,2048]{2,1,0:T(8,128)(2,1)}, u32[]{:S(2)}, u32[]{:S(2)}) async-start(bf16[16,8,2048]{2,1,0:T(8,128)(2,1)} %fusion.31), calls=%async_computation.5 | async-start | bytes 1048576 | tf_op jit(solution)/shard_map/all_to_all | solution.py:127
  129.7 14.1 %all-to-all-start.2 = ((bf16[4,64,2048]{2,1,0:T(8,128)(2,1)}), bf16[4,64,2048]{2,1,0:T(8,128)(2,1)}, u32[]{:S(2)}, u32[]{:S(2)}) async-start(bf16[4,64,2048]{2,1,0:T(8,128)(2,1)} %bitcast.135), calls=%async_computation.2 | async-start | bytes 2097152 | tf_op jit(solution)/shard_map/all_to_all | solution.py:18
  143.8 22.5 %all-to-all-start.5 = ((bf16[4,128,2048]{2,1,0:T(8,128)(2,1)}), bf16[4,128,2048]{2,1,0:T(8,128)(2,1)}, u32[]{:S(2)}, u32[]{:S(2)}) async-start(bf16[4,128,2048]{2,1,0:T(8,128)(2,1)} %bitcast.133), calls=%async_computation.6 | async-start | bytes 4194304 | tf_op jit(solution)/shard_map/all_to_all | solution.py:18
  148.3 117.6 %reduce-scatter.4.cloned.1.call-start = ((), (), s32[]{:S(2)}) async-start(), calls=%async_computation.13 | async-start | bytes 1310720 | tf_op jit(solution)/shard_map/reduce_scatter | solution.py:138
  166.3 46.0 %all-to-all-start.7 = ((bf16[16,8,2048]{2,1,0:T(8,128)(2,1)}), bf16[16,8,2048]{2,1,0:T(8,128)(2,1)}, u32[]{:S(2)}, u32[]{:S(2)}) async-start(bf16[16,8,2048]{2,1,0:T(8,128)(2,1)} %fusion.32), calls=%async_computation.9 | async-start | bytes 1048576 | tf_op jit(solution)/shard_map/all_to_all | solution.py:127
  190.9 108.3 %reduce-scatter.6.cloned.1.call-start = ((), (), s32[]{:S(2)}) async-start(), calls=%async_computation.14 | async-start | bytes 2621440 | tf_op jit(solution)/shard_map/reduce_scatter | solution.py:138
  205.1 105.9 %reduce-scatter.8.cloned.1.call-start = ((), (), s32[]{:S(2)}) async-start(), calls=%async_computation.15 | async-start | bytes 2621440 | tf_op jit(solution)/shard_map/reduce_scatter | solution.py:138
  214.3 40.3 %copy-start.22 = (bf16[1,2048,768]{2,1,0:T(8,128)(2,1)S(1)}, bf16[1,2048,768]{2,1,0:T(8,128)(2,1)}, u32[]{:S(2)}) copy-start(bf16[1,2048,768]{2,1,0:T(8,128)(2,1)} %param.27) | copy-start | bytes 9437188
  253.3 1.3 copy-start.4
  299.2 47.2 %copy-start.12 = (pred[16,2,2,128]{3,2,1,0:T(4,128)(4,1)S(1)}, pred[16,2,2,128]{3,2,1,0:T(4,128)(4,1)}, u32[]{:S(2)}) copy-start(pred[16,2,2,128]{3,2,1,0:T(4,128)(4,1)} %copy-done.11) | copy-start | bytes 24580
  299.2 47.2 %copy-start.19 = (pred[2,2]{1,0:T(4,128)(4,1)S(1)}, pred[2,2]{1,0:T(4,128)(4,1)}, u32[]{:S(2)}) copy-start(pred[2,2]{1,0:T(4,128)(4,1)} %copy-done.18) | copy-start | bytes 16
  299.2 34.6 %all-to-all-start.6 = ((bf16[16,8,2048]{2,1,0:T(8,128)(2,1)}), bf16[16,8,2048]{2,1,0:T(8,128)(2,1)}, u32[]{:S(2)}, u32[]{:S(2)}) async-start(bf16[16,8,2048]{2,1,0:T(8,128)(2,1)} %bitcast.139), calls=%async_computation.8 | async-start | bytes 1048576 | tf_op jit(solution)/shard_map/all_to_all | solution.py:142
  333.9 35.4 %all-to-all-start.9 = ((bf16[16,8,2048]{2,1,0:T(8,128)(2,1)}), bf16[16,8,2048]{2,1,0:T(8,128)(2,1)}, u32[]{:S(2)}, u32[]{:S(2)}) async-start(bf16[16,8,2048]{2,1,0:T(8,128)(2,1)} %bitcast.140), calls=%async_computation.12 | async-start | bytes 1048576 | tf_op jit(solution)/shard_map/all_to_all | solution.py:142
  348.2 2.6 copy-start.10
  348.2 5.4 %copy-start.9 = (bf16[16,2,4,2,128]{4,3,2,1,0:T(2,128)(2,1)S(1)}, bf16[16,2,4,2,128]{4,3,2,1,0:T(2,128)(2,1)}, u32[]{:S(2)}) copy-start(bf16[16,2,4,2,128]{4,3,2,1,0:T(2,128)(2,1)} %get-tuple-element.21) | copy-start | bytes 196612
  369.3 3.2 copy-start.1
  369.3 3.2 copy-start.2
  369.3 3.2 copy-start.13
  375.0 9.6 %copy-start.7 = (bf16[128,2048]{1,0:T(8,128)(2,1)S(1)}, bf16[128,2048]{1,0:T(8,128)(2,1)}, u32[]{:S(2)}) copy-start(bf16[128,2048]{1,0:T(8,128)(2,1)} %copy-done.5) | copy-start | bytes 1572868
  375.1 10.1 %copy-start.16 = (f32[2048]{0:T(1024)S(1)}, f32[2048]{0:T(1024)}, u32[]{:S(2)}) copy-start(f32[2048]{0:T(1024)} %param.31) | copy-start | bytes 24580
  375.1 10.1 %copy-start.17 = (f32[2048]{0:T(1024)S(1)}, f32[2048]{0:T(1024)}, u32[]{:S(2)}) copy-start(f32[2048]{0:T(1024)} %param.30) | copy-start | bytes 24580
  375.1 9.4 %collective-permute-start.3 = (f32[128,2048]{1,0:T(8,128)S(1)}, f32[128,2048]{1,0:T(8,128)S(1)}, u32[]{:S(2)}, u32[]{:S(2)}) collective-permute-start(f32[128,2048]{1,0:T(8,128)S(1)} %slice.71), channel_id=1, source_target_pairs={{0,4},{4,0},{1,5},{5,1},{2,6},{6,2},{3,7},{7,3},{8,12},{12,8},{9,1... | collective-permute-start | bytes 3145736 | tf_op jit(solution)/shard_map/ppermute | solution.py:27
Sparse Core Ops, SparseCore 0:
  158.2 36.8 reduce-scatter.3
  205.2 55.6 reduce-scatter.5
  266.0 44.0 reduce-scatter.7
